TPU v7x, 32 devices: a whole 2x2x4 slice. The times are simulated.
32 devices in a mesh: sp: 8 (over z, core), tp: 4 (over y, x).
Axes of the slice: x: 2, y: 2, z: 4, core: 2. Of those that a mesh axis runs over, the one named last changes fastest.
Arguments:
- residual_in: bfloat16 [2048, 2048], P(('sp', 'tp')), may hold values from -6 to 6
- query_a: bfloat16 [2048, 1024], P('sp', 'tp'), may hold values from -12 to 12
- key_a: bfloat16 [2048, 1024], P('sp', 'tp'), may hold values from -12 to 12
- value_a: bfloat16 [2048, 1024], P('sp', 'tp'), may hold values from -6 to 6
- query_b: bfloat16 [2048, 2048], P('sp', 'tp'), may hold values from -12 to 12
- key_b: bfloat16 [2048, 2048], P('sp', 'tp'), may hold values from -12 to 12
- value_b: bfloat16 [2048, 2048], P('sp', 'tp'), may hold values from -6 to 6
- cum_gates: float32 [2048, 2, 16], P('sp', None, 'tp'), may hold values from -247.76 to 0, as said below
- out_a: bfloat16 [1024, 2048], P('tp'), may hold values from -0.1875 to 0.1875
- out_b: bfloat16 [2048, 2048], P('tp'), may hold values from -0.125 to 0.125
- post_gain: bfloat16 [2048], replicated, may hold values from 0.099609375 to 1.8984375
- pre_gain: bfloat16 [2048], replicated, may hold values from 0.099609375 to 1.8984375
- expert_ids: int32 [2048, 2], P('sp'), may hold values from 0 to 7, all different within a row; in each aligned block of 256 rows (0 to 255, 256 to 511, ...) at most 80 rows name the same one
- expert_weights: float32 [2048, 2], P('sp'), may hold values from 0.2 to 1
- w_gate: bfloat16 [8, 2048, 4096], P('sp', None, 'tp'), may hold values from -0.125 to 0.125
- w_up: bfloat16 [8, 2048, 4096], P('sp', None, 'tp'), may hold values from -0.125 to 0.125
- w_down: bfloat16 [8, 4096, 2048], P('sp', 'tp'), may hold values from -0.09375 to 0.09375
Outputs:
- layer_out: bfloat16 [2048, 2048], P(('sp', 'tp'))
Inputs may be any that keep to these rules, and one draw needn't show every extreme that they name: `expert_ids`: in each aligned block of 256 positions no expert is named by more than 80 routes, a bound that some block reaches; a token's experts differ. `cum_gates`: never rises along the positions.
All inputs are finite; a program needn't handle non-finite values.
Results may differ from a plain program's by a relative error of at most 0.015.
Values may be sent and summed in bfloat16 or wider, within the bound.
A program may use at most 64 MiB of HBM per device.

v0:
```python
import jax
import jax.numpy as jnp
from jax import lax
from jax.sharding import PartitionSpec as P

eps_norm = 1e-06
big_neg = -1e30


def rms_scale(values, gain):
    return values * lax.rsqrt(jnp.mean(values * values, axis=-1, keepdims=True) + eps_norm) * gain


def empty_state(item_count, heads, width):
    return (
        jnp.full((heads, item_count), big_neg, jnp.float32),
        jnp.zeros((heads, item_count), jnp.float32),
        jnp.zeros((heads, item_count, width), jnp.float32),
    )


def update_state(state, query, key_rows, values, query_gate, key_gate, mask, width):
    highest, total, accum = state
    score = jnp.einsum(
        "rhd,khd->hrk", query, key_rows, preferred_element_type=jnp.float32
    ) * width ** (-0.5)
    score = score + query_gate.T[:, :, None] - key_gate.T[:, None, :]
    new_high = jnp.maximum(highest, jnp.max(jnp.where(mask[None], score, big_neg), axis=2))
    expo = jnp.exp(jnp.where(mask[None], score - new_high[:, :, None], big_neg))
    total = jnp.sum(expo, axis=2)
    accum = jnp.einsum(
        "hrk,khd->hrd", expo.astype(jnp.bfloat16), values, preferred_element_type=jnp.float32
    )
    return (new_high, total, accum)


def finish(state):
    highest, total, accum = state
    heads, item_count, width = accum.shape
    result = accum / total[:, :, None]
    return result.transpose(1, 0, 2).reshape(item_count, heads * width).astype(jnp.bfloat16)


def per_device(
    residual_in,
    query_a,
    key_a,
    value_a,
    query_b,
    key_b,
    value_b,
    cum_gates,
    out_a,
    out_b,
    post_gain,
    pre_gain,
    expert_ids,
    expert_weights,
    w_gate,
    w_up,
    w_down,
):
    rows = query_a.shape[0]
    heads = cum_gates.shape[2]
    width_a = query_a.shape[1] // heads
    width_b = query_b.shape[1] // heads
    group_size = lax.axis_size("sp")
    narrow = lax.axis_size("tp")
    here = lax.axis_index("sp")
    offset = here * rows
    gates_all = lax.all_gather(cum_gates, "sp", axis=0, tiled=True)
    queries_a = query_a.reshape(rows, heads, width_a)
    queries_b = query_b.reshape(rows, heads, width_b)
    blocks = [(queries_a, queries_b, offset + jnp.arange(rows, dtype=jnp.int32), cum_gates)]
    initial = tuple(
        (
            (
                empty_state(block[2].shape[0], heads, width_a),
                empty_state(block[2].shape[0], heads, width_b),
            )
            for block in blocks
        )
    )
    start = jnp.int32(0)
    piece_key_a = lax.all_gather(key_a.reshape(rows, heads, width_a), "sp", axis=0, tiled=True)
    piece_value_a = lax.all_gather(value_a.reshape(rows, heads, width_a), "sp", axis=0, tiled=True)
    piece_key_b = lax.all_gather(key_b.reshape(rows, heads, width_b), "sp", axis=0, tiled=True)
    piece_value_b = lax.all_gather(value_b.reshape(rows, heads, width_b), "sp", axis=0, tiled=True)
    item_count = piece_key_a.shape[0]
    key_pos = jnp.arange(item_count, dtype=jnp.int32)
    updated = []
    for state, (block_a, block_b, position, block_gate) in zip(initial, blocks):

        def compute(current):
            mask = key_pos[None, :] <= position[:, None]
            return (
                update_state(
                    current[0],
                    block_a,
                    piece_key_a,
                    piece_value_a,
                    block_gate[:, 0, :],
                    gates_all[:, 0, :],
                    mask,
                    width_a,
                ),
                update_state(
                    current[1],
                    block_b,
                    piece_key_b,
                    piece_value_b,
                    block_gate[:, 1, :],
                    gates_all[:, 1, :],
                    mask,
                    width_b,
                ),
            )

        updated.append(lax.cond(start <= position[-1], compute, lambda current: current, state))
    folded = tuple(updated)
    attn_a = finish(folded[0][0])
    attn_b = finish(folded[0][1])
    proj = lax.psum_scatter(
        (
            jnp.dot(attn_a, out_a, preferred_element_type=jnp.float32)
            + jnp.dot(attn_b, out_b, preferred_element_type=jnp.float32)
        ).astype(jnp.bfloat16),
        "tp",
        scatter_dimension=0,
        tiled=True,
    )
    post = rms_scale(proj.astype(jnp.float32), post_gain.astype(jnp.float32))
    mid_stream = (residual_in.astype(jnp.float32) + post).astype(jnp.bfloat16)
    normed = rms_scale(mid_stream.astype(jnp.float32), pre_gain.astype(jnp.float32)).astype(
        jnp.bfloat16
    )
    selected_count = expert_ids.shape[1]
    columns = normed.shape[1] // narrow
    slots = rows * selected_count * 5 // (4 * group_size)
    flat_experts = expert_ids.reshape(-1)
    onehot = (flat_experts[:, None] == jnp.arange(group_size, dtype=jnp.int32)[None, :]).astype(
        jnp.int32
    )
    rank = jnp.sum((jnp.cumsum(onehot, axis=0) - onehot) * onehot, axis=1)
    target = flat_experts * slots + rank
    owner = jnp.arange(rows * selected_count, dtype=jnp.int32) // selected_count
    table = jnp.full((group_size * slots,), -1, jnp.int32).at[target].set(owner)
    live = table >= 0
    source = jnp.maximum(table, 0)
    weighting = jnp.sum(
        expert_weights[:, :, None]
        * (
            target.reshape(rows, selected_count)[:, :, None]
            == jnp.arange(group_size * slots, dtype=jnp.int32)[None, None, :]
        ),
        axis=1,
    )
    column_rows = lax.all_to_all(normed, "tp", split_axis=1, concat_axis=0, tiled=True)
    outgoing = jnp.where(live[:, None], column_rows[source], jnp.zeros((), jnp.bfloat16))
    outgoing = outgoing.reshape(group_size, slots, columns)
    arrived = lax.all_to_all(outgoing, "sp", split_axis=0, concat_axis=0, tiled=True)
    flat = arrived.reshape(-1, columns)
    piece = lax.all_gather(flat, "tp", axis=1, tiled=True)
    gate_rows = w_gate[0]
    up_rows = w_up[0]
    gate = jnp.dot(piece, gate_rows, preferred_element_type=jnp.float32)
    upward = jnp.dot(piece, up_rows, preferred_element_type=jnp.float32)
    hidden_rows = (jax.nn.silu(gate) * upward).astype(jnp.bfloat16)
    hidden = hidden_rows.reshape(arrived.shape[0], arrived.shape[1], -1)
    flat_hidden = hidden.reshape(-1, hidden.shape[2])
    down_cols = w_down[0]
    summed = lax.psum_scatter(
        lax.dot_general(
            down_cols, flat_hidden, (((0,), (1,)), ((), ())), preferred_element_type=jnp.float32
        ).astype(jnp.bfloat16),
        "tp",
        scatter_dimension=0,
        tiled=True,
    )
    returned = lax.all_to_all(
        summed.reshape(columns, group_size, slots), "sp", split_axis=1, concat_axis=1, tiled=True
    )
    mixture_cols = jnp.einsum(
        "te,ce->tc",
        weighting,
        returned.reshape(columns, group_size * slots).astype(jnp.float32),
        precision=lax.Precision.HIGHEST,
    )
    mixture = lax.all_to_all(
        mixture_cols.astype(jnp.bfloat16), "tp", split_axis=0, concat_axis=1, tiled=True
    ).astype(mixture_cols.dtype)
    return (mid_stream.astype(jnp.float32) + mixture).astype(jnp.bfloat16)


def solution(mesh):
    placed = (
        P(("sp", "tp"), None),
        P("sp", "tp"),
        P("sp", "tp"),
        P("sp", "tp"),
        P("sp", "tp"),
        P("sp", "tp"),
        P("sp", "tp"),
        P("sp", None, "tp"),
        P("tp", None),
        P("tp", None),
        P(),
        P(),
        P("sp", None),
        P("sp", None),
        P("sp", None, "tp"),
        P("sp", None, "tp"),
        P("sp", "tp", None),
    )
    return jax.shard_map(
        per_device, mesh=mesh, in_specs=placed, out_specs=P(("sp", "tp"), None), check_vma=False
    )
```

profile of v0, /device:TPU:0, one launch (start us, length us, event | category | flops | bytes accessed | tf_op | source)
XLA Modules:
  0.0 352.2 jit_solution(581141033529459929)
XLA Ops:
  6.5 1.8 copy.59
  8.3 0.0 all-gather.6.cloned.1.call-update
  8.4 0.0 all-gather.8.cloned.1.call-start
  8.4 1.7 copy.60
  10.1 0.0 all-gather.8.cloned.1.call-update
  10.1 0.0 all-gather.10.cloned.1.call-start
  10.2 1.8 copy.61
  11.9 0.0 all-gather.10.cloned.1.call-update
  12.0 0.0 all-gather.12.cloned.1.call-start
  12.0 1.8 copy.62
  13.8 0.0 all-gather.12.cloned.1.call-update
  13.8 0.0 reduce-scatter.3.cloned.1.call-start
  13.9 0.6 slice.21
  15.0 16.0 %all_gather.19 = f32[2048,2,4]{0,2,1:T(4,128)S(1)} all-gather(f32[256,2,4]{0,2,1:T(4,128)} %param.26), channel_id=1, replica_groups=mesh['sp'=8,'tp'=4] {'sp'}, dimensions={0}, use_global_device_ids=true | all-gather | bytes 73728 | tf_op jit(solution)/shard_map/all_gather | solution.py:71
  31.0 4.8 %all-gather.6.cloned.1.call-done = bf16[2048,4,64]{0,2,1:T(8,128)(2,1)} async-done(((bf16[256,4,64]{0,2,1:T(8,128)(2,1)}), bf16[2048,4,64]{0,2,1:T(8,128)(2,1)}) %all-gather.6.cloned.1.call-update) | async-done | bytes 1048592 | tf_op jit(solution)/shard_map/all_gather | solution.py:85
  35.9 25.3 %all-gather.8.cloned.1.call-done = bf16[2048,4,64]{0,2,1:T(8,128)(2,1)} async-done(((bf16[256,4,64]{0,2,1:T(8,128)(2,1)}), bf16[2048,4,64]{0,2,1:T(8,128)(2,1)}) %all-gather.8.cloned.1.call-update) | async-done | bytes 1048592 | tf_op jit(solution)/shard_map/all_gather | solution.py:86
  61.2 31.0 %all-gather.10.cloned.1.call-done = bf16[2048,4,128]{0,2,1:T(8,128)(2,1)} async-done(((bf16[256,4,128]{0,2,1:T(8,128)(2,1)}), bf16[2048,4,128]{0,2,1:T(8,128)(2,1)}) %all-gather.10.cloned.1.call-update) | async-done | bytes 2097168 | tf_op jit(solution)/shard_map/all_gather | solution.py:87
  92.2 31.1 %all-gather.12.cloned.1.call-done = bf16[2048,4,128]{0,2,1:T(8,128)(2,1)} async-done(((bf16[256,4,128]{0,2,1:T(8,128)(2,1)}), bf16[2048,4,128]{0,2,1:T(8,128)(2,1)}) %all-gather.12.cloned.1.call-update) | async-done | bytes 2097168 | tf_op jit(solution)/shard_map/all_gather | solution.py:88
  123.3 22.6 %conditional.1 = (f32[4,256]{1,0:T(4,128)S(1)}, f32[4,256,64]{1,2,0:T(8,128)S(1)}, f32[4,256]{1,0:T(4,128)S(1)}, f32[4,256,128]{1,2,0:T(8,128)S(1)}) conditional(s32[]{:T(128)} %bitcast.9, () %tuple.13, (s32[2048]{0:T(1024)S(1)}, s32[256]{0:T(256)S(1)}, bf16[256,256]{1,0:T(8,128)(2,1)}, bf16[2048,4,64]{0,2,1:T(8,128)(2,1)}, f32[256,2,4]{0,2,1:T(4,128)}, ...), branch_computations={%region_0.0_spmd, %region_1.6_spmd} | conditional | flops 1682438144 | bytes 83133552 | solution.py:119
  123.3 0.7 slice_bitcast_fusion.3
  124.0 1.0 copy.63
  125.1 0.4 broadcast_compare_fusion
  125.4 2.7 fusion.53
  128.2 4.5 %select_reduce_fusion = (f32[4,256]{1,0:T(4,128)S(1)}, f32[4,256]{1,0:T(4,128)S(1)}, f32[4,256,2048]{2,1,0:T(8,128)S(1)}) fusion(f32[4,2048]{1,0:T(4,128)S(1)} %get-tuple-element.97, f32[4,256]{1,0:T(4,128)S(1)} %get-tuple-element.99, pred[256,2048]{1,0:T(8,128)(4,1)S(1)} %broadcast_compare_fusion, f32[4,2048]{1,0:T(4,128)S(1)} %get-tuple-element.96, ...), kind=kOutput, calls=%fused_computation.3 | convolution fusion | flops 557840384 | bytes 19742720 | tf_op jit(solution)/shard_map/cond/branch_1_fun/rhd,khd->hrk/dot_general | solution.py:24
  132.7 2.8 fusion.6
  135.5 5.9 %fusion.3 = (f32[4,256]{1,0:T(4,128)S(1)}, f32[4,256]{1,0:T(4,128)S(1)}) fusion(f32[4,256,2048]{2,1,0:T(8,128)S(1)} %get-tuple-element.100, f32[4,256]{1,0:T(4,128)S(1)} %get-tuple-element.101, f32[4,2048]{1,0:T(4,128)S(1)} %get-tuple-element.97, f32[4,256]{1,0:T(4,128)S(1)} %get-tuple-element.99, pred[256,2048]{1,0:T(8,128)(4,1)S(1)} %broadcast_compare_fusion, ...), kind=kLoop, calls=%fused_computation.11 | loop fusion | flops 25163776 | bytes 17391616 | tf_op jit(solution)/shard_map/cond/branch_1_fun/reduce_sum | solution.py:30
  141.4 4.3 %fusion.4 = f32[4,256,128]{1,2,0:T(8,128)S(1)} fusion(bf16[2048,4,128]{0,2,1:T(8,128)(2,1)} %get-tuple-element.88, f32[4,256,2048]{2,1,0:T(8,128)S(1)} %get-tuple-element.100, f32[4,256]{1,0:T(4,128)S(1)} %get-tuple-element.101, f32[4,2048]{1,0:T(4,128)S(1)} %get-tuple-element.97, f32[4,256]{1,0:T(4,128)S(1)} %get-tuple-element.99, ...), kind=kOutput, calls=%fused_computation.12 | convolution fusion | flops 549453824 | bytes 11575296 | tf_op jit(solution)/shard_map/cond | solution.py:119
  146.0 1.7 fusion.54
  147.8 1.7 fusion.29
  149.5 0.1 copy.67
  149.7 0.1 eq.42
  149.8 0.1 eq.38
  150.0 1.1 reduce-window.6
  151.1 0.2 slice_reduce_fusion
  151.4 0.1 fusion.43
  151.5 0.1 reduce_sum.60
  151.7 0.1 mul.94
  151.8 2.4 scatter_custom_fusion
  154.3 22.3 %reduce-scatter.3.cloned.1.call-done = bf16[64,2048]{1,0:T(8,128)(2,1)} async-done(((bf16[256,2048]{1,0:T(8,128)(2,1)}), bf16[64,2048]{1,0:T(8,128)(2,1)}) %reduce-scatter.3.cloned.1.call-update) | async-done | bytes 262160 | tf_op jit(solution)/shard_map/reduce_scatter | solution.py:123
  176.6 1.1 fusion.34
  177.8 1.3 fusion.38
  179.0 0.7 copy-done.1
  179.7 0.1 fusion.40
  179.9 0.7 copy.87
  180.6 3.4 all-to-all-start
  184.0 0.0 all-gather.14.cloned.1.call-start
  184.1 0.1 broadcast_in_dim.74
  184.2 5.3 %all-to-all-done = bf16[64,4,512]{2,0,1:T(8,128)(2,1)S(1)} async-done(((bf16[64,4,512]{2,0,1:T(8,128)(2,1)}), bf16[64,4,512]{2,0,1:T(8,128)(2,1)S(1)}, u32[]{:S(2)}, u32[]{:S(2)}) %all-to-all-start) | async-done | bytes 262176 | tf_op jit(solution)/shard_map/all_to_all | solution.py:158
  189.5 2.8 gather_fusion
  192.2 0.2 broadcast_select_fusion
  192.4 22.6 %all_to_all.42 = bf16[8,80,512]{2,1,0:T(8,128)(2,1)} all-to-all(bf16[8,80,512]{2,1,0:T(8,128)(2,1)S(1)} %broadcast_select_fusion), channel_id=1, replica_groups=mesh['sp'=8,'tp'=4] {'sp'}, dimensions={0} | all-to-all | bytes 1310720 | tf_op jit(solution)/shard_map/all_to_all | solution.py:161
  215.0 0.0 all-gather.14.cloned.1.call-update
  215.1 0.0 reduce-scatter.5.cloned.1.call-start
  215.1 37.2 %all-gather.14.cloned.1.call-done = bf16[640,2048]{1,0:T(8,128)(2,1)} async-done(((bf16[640,512]{1,0:T(8,128)(2,1)}), bf16[640,2048]{1,0:T(8,128)(2,1)}) %all-gather.14.cloned.1.call-update) | async-done | bytes 2621456 | tf_op jit(solution)/shard_map/all_gather | solution.py:163
  252.4 7.4 %fusion.19 = f32[640,1024]{1,0:T(8,128)} fusion(bf16[640,2048]{1,0:T(8,128)(2,1)} %all-gather.14.cloned.1.call-done, bf16[1,2048,1024]{2,1,0:T(8,128)(2,1)} %param.34), kind=kOutput, calls=%fused_computation.32 | convolution fusion | flops 2684354560 | bytes 9437184 | tf_op jit(solution)/shard_map/dot_general | solution.py:167
  259.7 12.3 %fusion.26 = bf16[2048,640]{0,1:T(8,128)(2,1)} fusion(bf16[1,1024,2048]{2,1,0:T(8,128)(2,1)} %param.35, f32[640,1024]{1,0:T(8,128)} %fusion.19, bf16[640,2048]{1,0:T(8,128)(2,1)} %all-gather.14.cloned.1.call-done, bf16[1,2048,1024]{2,1,0:T(8,128)(2,1)} %param.33), kind=kOutput, calls=%fused_computation.37 | convolution fusion | flops 5373952000 | bytes 16252928 | tf_op jit(solution)/shard_map/dot_general | solution.py:173
  272.0 39.7 %reduce-scatter.5.cloned.1.call-done = bf16[512,640]{0,1:T(8,128)(2,1)} async-done(((bf16[2048,640]{0,1:T(8,128)(2,1)}), bf16[512,640]{0,1:T(8,128)(2,1)}) %reduce-scatter.5.cloned.1.call-update) | async-done | bytes 655376 | tf_op jit(solution)/shard_map/reduce_scatter | solution.py:172
  311.8 4.6 %all-to-all-start.2 = ((bf16[512,8,80]{0,2,1:T(8,128)(2,1)}), bf16[512,8,80]{0,2,1:T(8,128)(2,1)S(1)}, u32[]{:S(2)}, u32[]{:S(2)}) async-start(bf16[512,8,80]{0,2,1:T(8,128)(2,1)} %bitcast.106), calls=%async_computation.4 | async-start | bytes 1310720 | tf_op jit(solution)/shard_map/all_to_all | solution.py:180
  316.3 0.1 copy.70
  316.4 0.2 select_reduce_fusion.2
  316.7 17.8 %all-to-all-done.2 = bf16[512,8,80]{0,2,1:T(8,128)(2,1)S(1)} async-done(((bf16[512,8,80]{0,2,1:T(8,128)(2,1)}), bf16[512,8,80]{0,2,1:T(8,128)(2,1)S(1)}, u32[]{:S(2)}, u32[]{:S(2)}) %all-to-all-start.2) | async-done | bytes 655392 | tf_op jit(solution)/shard_map/all_to_all | solution.py:180
  334.5 0.8 convolution_convert_fusion
  335.3 8.3 %all_to_all.43 = bf16[4,64,512]{2,1,0:T(8,128)(2,1)S(1)} all-to-all(bf16[4,64,512]{2,1,0:T(8,128)(2,1)S(1)} %bitcast.104), channel_id=1, replica_groups=mesh['sp'=8,'tp'=4] {'tp'}, dimensions={0} | all-to-all | bytes 524288 | tf_op jit(solution)/shard_map/all_to_all | solution.py:189
  343.7 1.7 fusion.41
  (43 shorter events, 0.4 us)
Async XLA Ops:
  6.5 141.2 %copy-start = (bf16[512,2048]{1,0:T(8,128)(2,1)S(1)}, bf16[512,2048]{1,0:T(8,128)(2,1)}, u32[]{:S(2)}) copy-start(bf16[512,2048]{1,0:T(8,128)(2,1)} %param.28) | copy-start | bytes 6291460
  6.5 29.3 %all-gather.6.cloned.1.call-start = ((), (), s32[]{:S(2)}) async-start(), calls=%async_computation.6 | async-start | bytes 1179648 | tf_op jit(solution)/shard_map/all_gather | solution.py:85
  8.4 52.8 %all-gather.8.cloned.1.call-start = ((), (), s32[]{:S(2)}) async-start(), calls=%async_computation.7 | async-start | bytes 1179648 | tf_op jit(solution)/shard_map/all_gather | solution.py:86
  10.1 82.1 %all-gather.10.cloned.1.call-start = ((), (), s32[]{:S(2)}) async-start(), calls=%async_computation.8 | async-start | bytes 2359296 | tf_op jit(solution)/shard_map/all_gather | solution.py:87
  12.0 111.3 %all-gather.12.cloned.1.call-start = ((), (), s32[]{:S(2)}) async-start(), calls=%async_computation.9 | async-start | bytes 2359296 | tf_op jit(solution)/shard_map/all_gather | solution.py:88
  13.8 162.8 %reduce-scatter.3.cloned.1.call-start = ((), (), s32[]{:S(2)}) async-start(), calls=%async_computation.10 | async-start | bytes 1310720 | tf_op jit(solution)/shard_map/reduce_scatter | solution.py:123
  124.0 4.1 %copy-start.9 = (bf16[256,512]{1,0:T(8,128)(2,1)S(1)}, bf16[256,512]{1,0:T(8,128)(2,1)}, u32[]{:S(2)}) copy-start(bf16[256,512]{1,0:T(8,128)(2,1)} %get-tuple-element.48) | copy-start | bytes 786436 | tf_op jit(solution)/shard_map/cond
  125.1 3.1 copy-start.7
  128.2 4.5 %copy-start.8 = (bf16[2048,4,64]{0,2,1:T(8,128)(2,1)S(1)}, bf16[2048,4,64]{0,2,1:T(8,128)(2,1)}, u32[]{:S(2)}) copy-start(bf16[2048,4,64]{0,2,1:T(8,128)(2,1)} %get-tuple-element.33) | copy-start | bytes 3145732 | tf_op jit(solution)/shard_map/cond
  145.9 3.6 %copy-start.5 = (s32[256,2]{0,1:T(2,128)S(1)}, s32[256,2]{0,1:T(2,128)}, u32[]{:S(2)}) copy-start(s32[256,2]{0,1:T(2,128)} %param.31) | copy-start | bytes 6148
  146.0 4.0 %copy-start.3 = (bf16[2048]{0:T(1024)(128)(2,1)S(1)}, bf16[2048]{0:T(1024)(128)(2,1)}, u32[]{:S(2)}) copy-start(bf16[2048]{0:T(1024)(128)(2,1)} %param.29) | copy-start | bytes 12292
  146.0 4.0 %copy-start.4 = (bf16[2048]{0:T(1024)(128)(2,1)S(1)}, bf16[2048]{0:T(1024)(128)(2,1)}, u32[]{:S(2)}) copy-start(bf16[2048]{0:T(1024)(128)(2,1)} %param.30) | copy-start | bytes 12292
  146.0 31.7 %copy-start.2 = (bf16[64,2048]{1,0:T(8,128)(2,1)S(1)}, bf16[64,2048]{1,0:T(8,128)(2,1)}, u32[]{:S(2)}) copy-start(bf16[64,2048]{1,0:T(8,128)(2,1)} %param.19) | copy-start | bytes 786436
  179.0 0.7 copy-start.1
  180.6 8.9 %all-to-all-start = ((bf16[64,4,512]{2,0,1:T(8,128)(2,1)}), bf16[64,4,512]{2,0,1:T(8,128)(2,1)S(1)}, u32[]{:S(2)}, u32[]{:S(2)}) async-start(bf16[64,4,512]{2,0,1:T(8,128)(2,1)} %bitcast.94), calls=%async_computation.1 | async-start | bytes 524288 | tf_op jit(solution)/shard_map/all_to_all | solution.py:158
  184.0 68.3 %all-gather.14.cloned.1.call-start = ((), (), s32[]{:S(2)}) async-start(), calls=%async_computation.11 | async-start | bytes 3276800 | tf_op jit(solution)/shard_map/all_gather | solution.py:163
  215.1 96.7 %reduce-scatter.5.cloned.1.call-start = ((), (), s32[]{:S(2)}) async-start(), calls=%async_computation.12 | async-start | bytes 3276800 | tf_op jit(solution)/shard_map/reduce_scatter | solution.py:172
  259.7 56.7 %copy-start.6 = (f32[256,2]{0,1:T(2,128)S(1)}, f32[256,2]{0,1:T(2,128)}, u32[]{:S(2)}) copy-start(f32[256,2]{0,1:T(2,128)} %param.32) | copy-start | bytes 6148
  311.8 22.7 %all-to-all-start.2 = ((bf16[512,8,80]{0,2,1:T(8,128)(2,1)}), bf16[512,8,80]{0,2,1:T(8,128)(2,1)S(1)}, u32[]{:S(2)}, u32[]{:S(2)}) async-start(bf16[512,8,80]{0,2,1:T(8,128)(2,1)} %bitcast.106), calls=%async_computation.4 | async-start | bytes 1310720 | tf_op jit(solution)/shard_map/all_to_all | solution.py:180
Sparse Core Ops, SparseCore 0:
  8.9 26.9 all-gather.5
  37.5 23.6 all-gather.7
  62.8 29.3 all-gather.9
  93.6 29.6 all-gather.11
  149.6 26.9 reduce-scatter.2
  215.2 37.1 all-gather.13
  272.2 39.5 reduce-scatter.4
where the time goes:
time: 353 us; the launch traced here: 352 us
  waiting for transfers between devices  215 us (61%)
  blocking collectives  46.9 us (13%)
  matrix products  38.2 us (11%)
  local copies, waits for them, and re-layouts  17.2 us (5%)
  between operations  14.4 us (4%)
  other arithmetic  12.3 us (3%)
  starting transfers between devices  8.24 us (2%)
    reduce_scatter x1, waiting for transfers between devices, per_device(): lax.psum_scatter(lax.dot_general(down_cols, flat_hidden, (((0,), (1,)), (...  39.7 us
    all_gather x1, waiting for transfers between devices, per_device(): piece = lax.all_gather(flat, 'tp', axis=1, tiled=True)  37.2 us
    all_gather x1, waiting for transfers between devices, per_device(): lax.all_gather(value_b.reshape(rows, heads, width_b), 'sp', axis=0, tiled...  31.1 us
    all_gather x1, waiting for transfers between devices, per_device(): lax.all_gather(key_b.reshape(rows, heads, width_b), 'sp', axis=0, tiled=T...  31 us
    all_gather x1, waiting for transfers between devices, per_device(): lax.all_gather(value_a.reshape(rows, heads, width_a), 'sp', axis=0, tiled...  25.3 us
    all_to_all x1, blocking collectives, per_device(): lax.all_to_all(outgoing, 'sp', split_axis=0, concat_axis=0, tiled=True)  22.6 us
    reduce_scatter x1, waiting for transfers between devices, per_device(): lax.psum_scatter((jnp.dot(attn_a, out_a, preferred_element_type=jnp.float...  22.3 us
    all_to_all x1, waiting for transfers between devices, per_device(): lax.all_to_all(summed.reshape(columns, group_size, slots), 'sp', split_ax...  17.8 us
  transfers between devices with their start and end apart: 9, of which 9 were waited for; matrix products, arithmetic and copies ran while one was open for 3% of the time, Pallas kernels for 0%

commit v1 on v0

--- a/solution.py
+++ b/solution.py
@@ -177,8 +177,16 @@
         scatter_dimension=0,
         tiled=True,
     )
-    returned = lax.all_to_all(
-        summed.reshape(columns, group_size, slots), "sp", split_axis=1, concat_axis=1, tiled=True
+    returned = jnp.concatenate(
+        lax.all_to_all(
+            jnp.stack(
+                jnp.split(summed.reshape(columns, group_size, slots), lax.axis_size("sp"), axis=1)
+            ),
+            "sp",
+            0,
+            0,
+        ),
+        axis=1,
     )
     mixture_cols = jnp.einsum(
         "te,ce->tc",

time: 353 us -> 365 us (1.034)
  local copies, waits for them, and re-layouts: 17.2 us -> 29.4 us
    unnamed x19 -> x26, local copies, waits for them, and re-layouts: 7.91 us -> 18.6 us
where the time goes in v1:
time: 365 us; the launch traced here: 364 us
  waiting for transfers between devices  215 us (59%)
  blocking collectives  46.9 us (13%)
  matrix products  38.2 us (10%)
  local copies, waits for them, and re-layouts  29.4 us (8%)
  between operations  14.4 us (4%)
  other arithmetic  12.3 us (3%)
  starting transfers between devices  8.26 us (2%)
    reduce_scatter x1, waiting for transfers between devices, per_device(): lax.psum_scatter(lax.dot_general(down_cols, flat_hidden, (((0,), (1,)), (...  39.7 us
    all_gather x1, waiting for transfers between devices, per_device(): piece = lax.all_gather(flat, 'tp', axis=1, tiled=True)  37.2 us
    all_gather x1, waiting for transfers between devices, per_device(): lax.all_gather(value_b.reshape(rows, heads, width_b), 'sp', axis=0, tiled...  31.1 us
    all_gather x1, waiting for transfers between devices, per_device(): lax.all_gather(key_b.reshape(rows, heads, width_b), 'sp', axis=0, tiled=T...  31 us
    all_gather x1, waiting for transfers between devices, per_device(): lax.all_gather(value_a.reshape(rows, heads, width_a), 'sp', axis=0, tiled...  25.3 us
    all_to_all x1, blocking collectives, per_device(): lax.all_to_all(outgoing, 'sp', split_axis=0, concat_axis=0, tiled=True)  22.6 us
    reduce_scatter x1, waiting for transfers between devices, per_device(): lax.psum_scatter((jnp.dot(attn_a, out_a, preferred_element_type=jnp.float...  22.3 us
    unnamed x26, local copies, waits for them, and re-layouts  18.6 us
  transfers between devices with their start and end apart: 9, of which 9 were waited for; matrix products, arithmetic and copies ran while one was open for 3% of the time, Pallas kernels for 0%

profile of v1, /device:TPU:0, one launch (start us, length us, event | category | flops | bytes accessed | tf_op | source)
XLA Modules:
  0.0 364.4 jit_solution(5493891955284571159)
XLA Ops:
  6.5 1.8 copy.59
  8.4 0.0 all-gather.8.cloned.1.call-start
  8.4 1.7 copy.60
  10.2 1.8 copy.61
  12.0 1.8 copy.62
  13.8 0.0 reduce-scatter.3.cloned.1.call-start
  13.9 0.6 slice.21
  15.0 16.0 %all_gather.19 = f32[2048,2,4]{0,2,1:T(4,128)S(1)} all-gather(f32[256,2,4]{0,2,1:T(4,128)} %param.26), channel_id=1, replica_groups=mesh['sp'=8,'tp'=4] {'sp'}, dimensions={0}, use_global_device_ids=true | all-gather | bytes 73728 | tf_op jit(solution)/shard_map/all_gather | solution.py:71
  31.0 4.8 %all-gather.6.cloned.1.call-done = bf16[2048,4,64]{0,2,1:T(8,128)(2,1)} async-done(((bf16[256,4,64]{0,2,1:T(8,128)(2,1)}), bf16[2048,4,64]{0,2,1:T(8,128)(2,1)}) %all-gather.6.cloned.1.call-update) | async-done | bytes 1048592 | tf_op jit(solution)/shard_map/all_gather | solution.py:85
  35.9 25.3 %all-gather.8.cloned.1.call-done = bf16[2048,4,64]{0,2,1:T(8,128)(2,1)} async-done(((bf16[256,4,64]{0,2,1:T(8,128)(2,1)}), bf16[2048,4,64]{0,2,1:T(8,128)(2,1)}) %all-gather.8.cloned.1.call-update) | async-done | bytes 1048592 | tf_op jit(solution)/shard_map/all_gather | solution.py:86
  61.2 31.0 %all-gather.10.cloned.1.call-done = bf16[2048,4,128]{0,2,1:T(8,128)(2,1)} async-done(((bf16[256,4,128]{0,2,1:T(8,128)(2,1)}), bf16[2048,4,128]{0,2,1:T(8,128)(2,1)}) %all-gather.10.cloned.1.call-update) | async-done | bytes 2097168 | tf_op jit(solution)/shard_map/all_gather | solution.py:87
  92.2 31.1 %all-gather.12.cloned.1.call-done = bf16[2048,4,128]{0,2,1:T(8,128)(2,1)} async-done(((bf16[256,4,128]{0,2,1:T(8,128)(2,1)}), bf16[2048,4,128]{0,2,1:T(8,128)(2,1)}) %all-gather.12.cloned.1.call-update) | async-done | bytes 2097168 | tf_op jit(solution)/shard_map/all_gather | solution.py:88
  123.3 22.6 %conditional.1 = (f32[4,256]{1,0:T(4,128)S(1)}, f32[4,256,64]{1,2,0:T(8,128)S(1)}, f32[4,256]{1,0:T(4,128)S(1)}, f32[4,256,128]{1,2,0:T(8,128)S(1)}) conditional(s32[]{:T(128)} %bitcast.9, () %tuple.13, (s32[2048]{0:T(1024)S(1)}, s32[256]{0:T(256)S(1)}, bf16[256,256]{1,0:T(8,128)(2,1)}, bf16[2048,4,64]{0,2,1:T(8,128)(2,1)}, f32[256,2,4]{0,2,1:T(4,128)}, ...), branch_computations={%region_0.0_spmd, %region_1.6_spmd} | conditional | flops 1682438144 | bytes 83133552 | solution.py:119
  123.3 0.7 slice_bitcast_fusion.3
  124.0 1.0 copy.63
  125.1 0.4 broadcast_compare_fusion
  125.4 2.7 fusion.61
  128.2 4.5 %select_reduce_fusion = (f32[4,256]{1,0:T(4,128)S(1)}, f32[4,256]{1,0:T(4,128)S(1)}, f32[4,256,2048]{2,1,0:T(8,128)S(1)}) fusion(f32[4,2048]{1,0:T(4,128)S(1)} %get-tuple-element.97, f32[4,256]{1,0:T(4,128)S(1)} %get-tuple-element.99, pred[256,2048]{1,0:T(8,128)(4,1)S(1)} %broadcast_compare_fusion, f32[4,2048]{1,0:T(4,128)S(1)} %get-tuple-element.96, ...), kind=kOutput, calls=%fused_computation.3 | convolution fusion | flops 557840384 | bytes 19742720 | tf_op jit(solution)/shard_map/cond/branch_1_fun/rhd,khd->hrk/dot_general | solution.py:24
  132.7 2.8 fusion.6
  135.5 5.9 %fusion.3 = (f32[4,256]{1,0:T(4,128)S(1)}, f32[4,256]{1,0:T(4,128)S(1)}) fusion(f32[4,256,2048]{2,1,0:T(8,128)S(1)} %get-tuple-element.100, f32[4,256]{1,0:T(4,128)S(1)} %get-tuple-element.101, f32[4,2048]{1,0:T(4,128)S(1)} %get-tuple-element.97, f32[4,256]{1,0:T(4,128)S(1)} %get-tuple-element.99, pred[256,2048]{1,0:T(8,128)(4,1)S(1)} %broadcast_compare_fusion, ...), kind=kLoop, calls=%fused_computation.11 | loop fusion | flops 25163776 | bytes 17391616 | tf_op jit(solution)/shard_map/cond/branch_1_fun/reduce_sum | solution.py:30
  141.4 4.3 %fusion.4 = f32[4,256,128]{1,2,0:T(8,128)S(1)} fusion(bf16[2048,4,128]{0,2,1:T(8,128)(2,1)} %get-tuple-element.88, f32[4,256,2048]{2,1,0:T(8,128)S(1)} %get-tuple-element.100, f32[4,256]{1,0:T(4,128)S(1)} %get-tuple-element.101, f32[4,2048]{1,0:T(4,128)S(1)} %get-tuple-element.97, f32[4,256]{1,0:T(4,128)S(1)} %get-tuple-element.99, ...), kind=kOutput, calls=%fused_computation.12 | convolution fusion | flops 549453824 | bytes 11575296 | tf_op jit(solution)/shard_map/cond | solution.py:119
  146.0 1.7 fusion.62
  147.8 1.7 fusion.29
  149.5 0.1 copy.67
  149.7 0.1 eq.42
  149.8 0.1 eq.38
  150.0 1.1 reduce-window.6
  151.1 0.2 slice_reduce_fusion
  151.4 0.1 fusion.51
  151.5 0.1 reduce_sum.60
  151.7 0.1 mul.94
  151.8 2.4 scatter_custom_fusion
  154.3 22.3 %reduce-scatter.3.cloned.1.call-done = bf16[64,2048]{1,0:T(8,128)(2,1)} async-done(((bf16[256,2048]{1,0:T(8,128)(2,1)}), bf16[64,2048]{1,0:T(8,128)(2,1)}) %reduce-scatter.3.cloned.1.call-update) | async-done | bytes 262160 | tf_op jit(solution)/shard_map/reduce_scatter | solution.py:123
  176.6 1.1 fusion.34
  177.8 1.3 fusion.38
  179.0 0.7 copy-done.1
  179.7 0.1 fusion.40
  179.9 0.7 copy.87
  180.6 3.4 all-to-all-start
  184.1 0.1 broadcast_in_dim.74
  184.2 5.3 %all-to-all-done = bf16[64,4,512]{2,0,1:T(8,128)(2,1)S(1)} async-done(((bf16[64,4,512]{2,0,1:T(8,128)(2,1)}), bf16[64,4,512]{2,0,1:T(8,128)(2,1)S(1)}, u32[]{:S(2)}, u32[]{:S(2)}) %all-to-all-start) | async-done | bytes 262176 | tf_op jit(solution)/shard_map/all_to_all | solution.py:158
  189.5 2.8 gather_fusion
  192.2 0.2 broadcast_select_fusion
  192.4 22.6 %all_to_all.42 = bf16[8,80,512]{2,1,0:T(8,128)(2,1)} all-to-all(bf16[8,80,512]{2,1,0:T(8,128)(2,1)S(1)} %broadcast_select_fusion), channel_id=1, replica_groups=mesh['sp'=8,'tp'=4] {'sp'}, dimensions={0} | all-to-all | bytes 1310720 | tf_op jit(solution)/shard_map/all_to_all | solution.py:161
  215.1 0.0 reduce-scatter.5.cloned.1.call-start
  215.1 37.2 %all-gather.14.cloned.1.call-done = bf16[640,2048]{1,0:T(8,128)(2,1)} async-done(((bf16[640,512]{1,0:T(8,128)(2,1)}), bf16[640,2048]{1,0:T(8,128)(2,1)}) %all-gather.14.cloned.1.call-update) | async-done | bytes 2621456 | tf_op jit(solution)/shard_map/all_gather | solution.py:163
  252.4 7.4 %fusion.19 = f32[640,1024]{1,0:T(8,128)} fusion(bf16[640,2048]{1,0:T(8,128)(2,1)} %all-gather.14.cloned.1.call-done, bf16[1,2048,1024]{2,1,0:T(8,128)(2,1)} %param.34), kind=kOutput, calls=%fused_computation.32 | convolution fusion | flops 2684354560 | bytes 9437184 | tf_op jit(solution)/shard_map/dot_general | solution.py:167
  259.7 12.3 %fusion.26 = bf16[2048,640]{0,1:T(8,128)(2,1)} fusion(bf16[1,1024,2048]{2,1,0:T(8,128)(2,1)} %param.35, f32[640,1024]{1,0:T(8,128)} %fusion.19, bf16[640,2048]{1,0:T(8,128)(2,1)} %all-gather.14.cloned.1.call-done, bf16[1,2048,1024]{2,1,0:T(8,128)(2,1)} %param.33), kind=kOutput, calls=%fused_computation.37 | convolution fusion | flops 5373952000 | bytes 16252928 | tf_op jit(solution)/shard_map/dot_general | solution.py:173
  272.0 39.7 %reduce-scatter.5.cloned.1.call-done = bf16[512,640]{0,1:T(8,128)(2,1)} async-done(((bf16[2048,640]{0,1:T(8,128)(2,1)}), bf16[512,640]{0,1:T(8,128)(2,1)}) %reduce-scatter.5.cloned.1.call-update) | async-done | bytes 655376 | tf_op jit(solution)/shard_map/reduce_scatter | solution.py:172
  311.8 1.5 fusion.49
  313.3 1.5 fusion.48
  314.8 1.5 fusion.47
  316.3 1.5 fusion.46
  317.9 1.5 fusion.45
  319.4 1.5 fusion.44
  320.9 1.5 fusion.43
  322.4 1.5 fusion.42
  323.9 4.6 %all-to-all-start.2 = ((bf16[8,512,1,80]{1,3,2,0:T(8,128)(2,1)}), bf16[8,512,1,80]{1,3,2,0:T(8,128)(2,1)S(1)}, u32[]{:S(2)}, u32[]{:S(2)}) async-start(bf16[8,512,1,80]{1,3,2,0:T(8,128)(2,1)} %fusion.42), calls=%async_computation.4 | async-start | bytes 1310720 | tf_op jit(solution)/shard_map/all_to_all | solution.py:181
  328.6 0.1 copy.70
  328.6 0.2 select_reduce_fusion.2
  328.9 17.8 %all-to-all-done.2 = bf16[8,512,1,80]{1,3,2,0:T(8,128)(2,1)S(1)} async-done(((bf16[8,512,1,80]{1,3,2,0:T(8,128)(2,1)}), bf16[8,512,1,80]{1,3,2,0:T(8,128)(2,1)S(1)}, u32[]{:S(2)}, u32[]{:S(2)}) %all-to-all-start.2) | async-done | bytes 655392 | tf_op jit(solution)/shard_map/all_to_all | solution.py:181
  346.7 0.8 convolution_convert_fusion
  347.5 8.3 %all_to_all.43 = bf16[4,64,512]{2,1,0:T(8,128)(2,1)S(1)} all-to-all(bf16[4,64,512]{2,1,0:T(8,128)(2,1)S(1)} %bitcast.138), channel_id=1, replica_groups=mesh['sp'=8,'tp'=4] {'tp'}, dimensions={0} | all-to-all | bytes 524288 | tf_op jit(solution)/shard_map/all_to_all | solution.py:197
  355.8 1.7 fusion.41
  (51 shorter events, 0.6 us)
Async XLA Ops:
  6.5 141.2 %copy-start = (bf16[512,2048]{1,0:T(8,128)(2,1)S(1)}, bf16[512,2048]{1,0:T(8,128)(2,1)}, u32[]{:S(2)}) copy-start(bf16[512,2048]{1,0:T(8,128)(2,1)} %param.28) | copy-start | bytes 6291460
  6.5 29.3 %all-gather.6.cloned.1.call-start = ((), (), s32[]{:S(2)}) async-start(), calls=%async_computation.6 | async-start | bytes 1179648 | tf_op jit(solution)/shard_map/all_gather | solution.py:85
  8.4 52.8 %all-gather.8.cloned.1.call-start = ((), (), s32[]{:S(2)}) async-start(), calls=%async_computation.7 | async-start | bytes 1179648 | tf_op jit(solution)/shard_map/all_gather | solution.py:86
  10.1 82.1 %all-gather.10.cloned.1.call-start = ((), (), s32[]{:S(2)}) async-start(), calls=%async_computation.8 | async-start | bytes 2359296 | tf_op jit(solution)/shard_map/all_gather | solution.py:87
  12.0 111.3 %all-gather.12.cloned.1.call-start = ((), (), s32[]{:S(2)}) async-start(), calls=%async_computation.9 | async-start | bytes 2359296 | tf_op jit(solution)/shard_map/all_gather | solution.py:88
  13.8 162.8 %reduce-scatter.3.cloned.1.call-start = ((), (), s32[]{:S(2)}) async-start(), calls=%async_computation.10 | async-start | bytes 1310720 | tf_op jit(solution)/shard_map/reduce_scatter | solution.py:123
  124.0 4.1 %copy-start.9 = (bf16[256,512]{1,0:T(8,128)(2,1)S(1)}, bf16[256,512]{1,0:T(8,128)(2,1)}, u32[]{:S(2)}) copy-start(bf16[256,512]{1,0:T(8,128)(2,1)} %get-tuple-element.48) | copy-start | bytes 786436 | tf_op jit(solution)/shard_map/cond
  125.1 3.1 copy-start.7
  128.2 4.5 %copy-start.8 = (bf16[2048,4,64]{0,2,1:T(8,128)(2,1)S(1)}, bf16[2048,4,64]{0,2,1:T(8,128)(2,1)}, u32[]{:S(2)}) copy-start(bf16[2048,4,64]{0,2,1:T(8,128)(2,1)} %get-tuple-element.33) | copy-start | bytes 3145732 | tf_op jit(solution)/shard_map/cond
  145.9 3.6 copy-start.5
  146.0 4.0 %copy-start.3 = (bf16[2048]{0:T(1024)(128)(2,1)S(1)}, bf16[2048]{0:T(1024)(128)(2,1)}, u32[]{:S(2)}) copy-start(bf16[2048]{0:T(1024)(128)(2,1)} %param.29) | copy-start | bytes 12292
  146.0 4.0 %copy-start.4 = (bf16[2048]{0:T(1024)(128)(2,1)S(1)}, bf16[2048]{0:T(1024)(128)(2,1)}, u32[]{:S(2)}) copy-start(bf16[2048]{0:T(1024)(128)(2,1)} %param.30) | copy-start | bytes 12292
  146.0 31.7 %copy-start.2 = (bf16[64,2048]{1,0:T(8,128)(2,1)S(1)}, bf16[64,2048]{1,0:T(8,128)(2,1)}, u32[]{:S(2)}) copy-start(bf16[64,2048]{1,0:T(8,128)(2,1)} %param.19) | copy-start | bytes 786436
  179.0 0.7 copy-start.1
  180.6 8.9 %all-to-all-start = ((bf16[64,4,512]{2,0,1:T(8,128)(2,1)}), bf16[64,4,512]{2,0,1:T(8,128)(2,1)S(1)}, u32[]{:S(2)}, u32[]{:S(2)}) async-start(bf16[64,4,512]{2,0,1:T(8,128)(2,1)} %bitcast.128), calls=%async_computation.1 | async-start | bytes 524288 | tf_op jit(solution)/shard_map/all_to_all | solution.py:158
  184.0 68.3 %all-gather.14.cloned.1.call-start = ((), (), s32[]{:S(2)}) async-start(), calls=%async_computation.11 | async-start | bytes 3276800 | tf_op jit(solution)/shard_map/all_gather | solution.py:163
  215.1 96.7 %reduce-scatter.5.cloned.1.call-start = ((), (), s32[]{:S(2)}) async-start(), calls=%async_computation.12 | async-start | bytes 3276800 | tf_op jit(solution)/shard_map/reduce_scatter | solution.py:172
  272.0 56.6 %copy-start.6 = (f32[256,2]{0,1:T(2,128)S(1)}, f32[256,2]{0,1:T(2,128)}, u32[]{:S(2)}) copy-start(f32[256,2]{0,1:T(2,128)} %param.32) | copy-start | bytes 6148
  323.9 22.7 %all-to-all-start.2 = ((bf16[8,512,1,80]{1,3,2,0:T(8,128)(2,1)}), bf16[8,512,1,80]{1,3,2,0:T(8,128)(2,1)S(1)}, u32[]{:S(2)}, u32[]{:S(2)}) async-start(bf16[8,512,1,80]{1,3,2,0:T(8,128)(2,1)} %fusion.42), calls=%async_computation.4 | async-start | bytes 1310720 | tf_op jit(solution)/shard_map/all_to_all | solution.py:181
Sparse Core Ops, SparseCore 0:
  8.9 26.9 all-gather.5
  37.5 23.6 all-gather.7
  62.8 29.3 all-gather.9
  93.6 29.6 all-gather.11
  149.6 26.9 reduce-scatter.2
  215.2 37.1 all-gather.13
  272.2 39.5 reduce-scatter.4
